TPU v7x, 32 devices: a whole 2x2x4 slice. The times are simulated.
32 devices in a mesh: row: 8 (over z, core), col: 4 (over y, x).
Axes of the slice: x: 2, y: 2, z: 4, core: 2. Of those that a mesh axis runs over, the one named last changes fastest.
Arguments:
- tokens: bfloat16 [4096, 2048], P('row'), may hold values from -6 to 6
- out_weight: bfloat16 [2048, 2048], P(None, 'col'), may hold values from -0.125 to 0.125
Outputs:
- mixed: bfloat16 [4096, 2048], P('row', 'col')
All inputs are finite; a program needn't handle non-finite values.
Results may differ from a plain program's by a relative error of at most 0.001.
Values may be sent and summed in bfloat16 or wider, within the bound.
No kernel may reach another device: no remote copies, remote signals or barrier semaphores. Data moves between devices by JAX's collectives and lax.ppermute only.
A program may use at most 64 MiB of HBM per device.

v0:
```python
import math

import jax
import jax.numpy as jnp
import numpy as np
from jax import lax
from jax.experimental import pallas as pl
from jax.experimental.pallas import tpu as pltpu
from jax.sharding import PartitionSpec as P

GROUPS = 4
GROUP_DIM = 512
HALF = GROUP_DIM // 2
BF = jnp.bfloat16
F32 = jnp.float32


def two_parts(table):
    high = np.asarray(table, np.float32).astype(BF)
    low = (np.asarray(table, np.float64) - high.astype(np.float64)).astype(np.float32).astype(BF)
    return high, low


def split(value):
    high = value.astype(BF)
    return high, (value - high.astype(F32)).astype(BF)


def dot_nt(left, right):
    return lax.dot_general(left, right, (((1,), (1,)), ((), ())), preferred_element_type=F32)


def dot_nn(left, right):
    return jnp.dot(left, right, preferred_element_type=F32)


def position_kernel(x_ref, m_ref, tw_c, tw_s, th_ref, tl_ref, o_ref, lh_ref, ll_ref):
    rows, chans, seg = x_ref.shape
    pairs = chans // 2
    cols = o_ref.shape[1]
    kb = o_ref.shape[2]
    mask = m_ref[...]
    evens, odds = [], []
    for r in range(rows):
        block = x_ref[r].astype(F32)
        lo, hi = block[:pairs], block[pairs:]
        evens.append(lo + mask * hi)
        odds.append(mask * lo + (1.0 - 2.0 * mask) * hi)

    def combine(values, j):
        real, imag = None, None
        for r in range(rows):
            c = math.cos(2 * math.pi * ((r * j) % rows) / rows)
            s = -math.sin(2 * math.pi * ((r * j) % rows) / rows)
            for kind, w in (("r", c), ("i", s)):
                if abs(w) < 1e-9:
                    continue
                if abs(abs(w) - 1.0) < 1e-9:
                    term = values[r] if w > 0 else -values[r]
                else:
                    term = w * values[r]
                if kind == "r":
                    real = term if real is None else real + term
                else:
                    imag = term if imag is None else imag + term
        if imag is None:
            imag = jnp.zeros_like(real)
        return real, imag

    def place(at, left, right):
        for side, value in ((0, left), (seg, right)):
            high, low = split(value)
            lh_ref[at : at + pairs, side : side + seg] = high
            ll_ref[at : at + pairs, side : side + seg] = low

    for j0 in range(rows // 2 + 1):
        er, ei = combine(evens, j0)
        orr, oi = combine(odds, j0)
        for j, sign in ((j0, 1.0), (rows - j0, -1.0)):
            if j == rows or (sign < 0 and j == j0):
                continue
            c, s = tw_c[j : j + 1], tw_s[j : j + 1]
            ein, oin = sign * ei, sign * oi
            place(j * chans, er * c + ein * s, ein * c - er * s)
            tr, ti = orr * c + oin * s, oin * c - orr * s
            place(
                j * chans + pairs,
                (1.0 - mask) * tr - mask * ti,
                mask * tr + (1.0 - mask) * ti,
            )
    width = o_ref.shape[3]
    for c in range(cols):
        lh, ll = lh_ref[c * width : (c + 1) * width], ll_ref[c * width : (c + 1) * width]
        th = th_ref[...]
        z = dot_nt(th, lh) + dot_nt(th, ll) + dot_nt(tl_ref[...], lh)
        for r in range(rows):
            o_ref[r, c] = z[r * kb : (r + 1) * kb]


def output_kernel(at_ref, z_ref, gh_ref, gl_ref, mine_ref, other_ref, o_ref, zh_ref, zl_ref, sh_ref, sl_ref):
    rows, cols, kb, width = z_ref.shape
    step = pl.program_id(0)
    total = zh_ref.shape[1]
    chans = total // (rows * cols)
    jb = width // chans

    @pl.when(step == 0)
    def _():
        for c in range(cols):
            for r in range(rows):
                block = z_ref[r, c]
                high, low = split(block)
                lane = (c * rows + r) * chans
                for jj in range(jb):
                    zh_ref[jj * kb : (jj + 1) * kb, lane : lane + chans] = high[:, jj * chans : (jj + 1) * chans]
                    zl_ref[jj * kb : (jj + 1) * kb, lane : lane + chans] = low[:, jj * chans : (jj + 1) * chans]
        for g in range(GROUPS):
            cut = slice(g * GROUP_DIM, (g + 1) * GROUP_DIM)
            zh, zl = zh_ref[:, cut], zl_ref[:, cut]
            gh = gh_ref[...]
            spectral = dot_nn(zh, gh) + dot_nn(zl, gh) + dot_nn(zh, gl_ref[...])
            high, low = split(spectral)
            half, at = divmod(g * GROUP_DIM, total // 2)
            sh_ref[half, :, at : at + GROUP_DIM] = high
            sl_ref[half, :, at : at + GROUP_DIM] = low

    half = at_ref[0]
    mine, other = mine_ref[0], other_ref[0]
    result = dot_nn(sh_ref[half], mine) + dot_nn(sl_ref[half], mine)
    result = result + dot_nn(sh_ref[1 - half], other) + dot_nn(sl_ref[1 - half], other)
    o_ref[0] = result.astype(BF)


def body(tokens, out_weight):
    seg, dim = tokens.shape
    out_cols = out_weight.shape[1]
    rows = lax.axis_size("row")
    cols = lax.axis_size("col")
    row, col = lax.axis_index("row"), lax.axis_index("col")
    length = seg * rows
    chans = dim // (rows * cols)
    pairs = chans // 2
    jb, kb = rows // cols, seg // rows

    half = row % 2
    own = lax.dynamic_slice(out_weight, (half * (dim // 2), 0), (dim // 2, out_cols))
    rest = lax.dynamic_slice(out_weight, ((1 - half) * (dim // 2), 0), (dim // 2, out_cols))
    fetched = [
        lax.ppermute(own, "col", [(c, c ^ d) for c in range(cols)]) for d in range(1, cols)
    ]
    mine = jnp.stack([own] + fetched)
    swapped = [lax.ppermute(f, "row", [(r, r ^ 1) for r in range(rows)]) for f in fetched]
    other = jnp.stack([rest] + swapped)

    group = (col * GROUPS) // cols
    group_tokens = lax.dynamic_slice(tokens, (0, group * GROUP_DIM), (seg, GROUP_DIM))
    slot = jnp.arange(rows * chans, dtype=jnp.int32)
    pair = (col * rows + slot // chans) * pairs + (slot % chans) % pairs
    p = pair % HALF
    upper = (slot % chans) >= pairs
    channel = jnp.where(upper, jnp.where(p == 0, HALF, GROUP_DIM - p), p)
    pick = (channel[:, None] == jnp.arange(GROUP_DIM, dtype=jnp.int32)[None, :]).astype(BF)
    turned = dot_nt(pick, group_tokens).astype(BF).reshape(rows, chans, seg)
    whole = lax.all_to_all(turned, "row", split_axis=0, concat_axis=0, tiled=True)

    own_pair = (col * rows + row) * pairs + jnp.arange(pairs, dtype=jnp.int32)
    mask = ((own_pair % HALF) != 0).astype(F32)[:, None]
    s_at = np.arange(seg)
    twist = 2 * np.pi * ((np.arange(rows)[:, None] * s_at[None, :]) % length) / length
    phase = 2 * np.pi * ((s_at[:, None] * s_at[None, :]) % seg) / seg
    th, tl = two_parts(np.concatenate([np.cos(phase), np.sin(phase)], axis=1))
    spread = pl.pallas_call(
        position_kernel,
        out_shape=jax.ShapeDtypeStruct((rows, cols, kb, jb * chans), F32),
        scratch_shapes=[pltpu.VMEM((rows * chans, 2 * seg), BF)] * 2,
        name="positions",
    )(whole, mask, np.cos(twist).astype(np.float32), np.sin(twist).astype(np.float32), th, tl)
    flat = spread.reshape(rows * cols, kb, jb * chans)
    mixed_in = lax.all_to_all(flat, ("row", "col"), split_axis=0, concat_axis=0, tiled=True)
    mixed_in = mixed_in.reshape(rows, cols, kb, jb * chans)

    lanes = np.arange(GROUP_DIM)
    lp = (lanes // chans) * pairs + (lanes % chans) % pairs
    odd = (lanes % chans) >= pairs
    turn = 2 * np.pi * ((lp[:, None] * lanes[None, :]) % GROUP_DIM) / GROUP_DIM
    flip = np.where(lanes % 2 == 0, 1.0, -1.0)[None, :]
    grid_table = np.where(odd[:, None], np.where(lp[:, None] == 0, flip, -np.sin(turn)), np.cos(turn))
    gh, gl = two_parts(grid_table / math.sqrt(length * GROUP_DIM))
    places = jnp.stack([half, col]).astype(jnp.int32)
    few = jb * kb
    whole_spec = lambda shape: pl.BlockSpec(shape, lambda d, at: (0,) * len(shape))
    out = pl.pallas_call(
        output_kernel,
        out_shape=jax.ShapeDtypeStruct((cols, few, out_cols), BF),
        grid_spec=pltpu.PrefetchScalarGridSpec(
            num_scalar_prefetch=1,
            grid=(cols,),
            in_specs=[
                whole_spec(mixed_in.shape),
                whole_spec((GROUP_DIM, GROUP_DIM)),
                whole_spec((GROUP_DIM, GROUP_DIM)),
                pl.BlockSpec((1, dim // 2, out_cols), lambda d, at: (d, 0, 0)),
                pl.BlockSpec((1, dim // 2, out_cols), lambda d, at: (d, 0, 0)),
            ],
            out_specs=pl.BlockSpec((1, few, out_cols), lambda d, at: (jnp.bitwise_xor(d, at[1]), 0, 0)),
            scratch_shapes=[pltpu.VMEM((few, dim), BF)] * 2 + [pltpu.VMEM((2, few, dim // 2), BF)] * 2,
        ),
        name="outputs",
    )(places, mixed_in, gh, gl, mine, other)
    gathered = lax.all_to_all(out, "col", split_axis=0, concat_axis=0, tiled=True)
    gathered = gathered.reshape(seg, out_cols)
    at = jnp.arange(seg, dtype=jnp.int32)
    wanted = (at % rows) * kb + at // rows
    order = (wanted[:, None] == at[None, :]).astype(BF)
    return dot_nn(order, gathered).astype(BF)


def solution(mesh):
    placed = (P("row", None), P(None, "col"))
    return jax.shard_map(
        body, mesh=mesh, in_specs=placed, out_specs=P("row", "col"), check_vma=False
    )
```

profile of v0, /device:TPU:0, one launch (start us, length us, event | category | flops | bytes accessed | tf_op | source)
XLA Modules:
  0.0 100.6 jit_solution(17416169535605158165)
XLA Ops:
  0.0 1.6 %copy-done = bf16[512,2048]{1,0:T(8,128)(2,1)S(1)} copy-done((bf16[512,2048]{1,0:T(8,128)(2,1)S(1)}, bf16[512,2048]{1,0:T(8,128)(2,1)}, u32[]{:S(2)}) %copy-start) | copy-done | bytes 2097176
  1.6 1.3 %convolution_convert_fusion.1 = bf16[512,512]{1,0:T(8,128)(2,1)} fusion(bf16[512,2048]{1,0:T(8,128)(2,1)S(1)} %copy-done, s32[]{:T(128)S(6)} %select_n.112, s32[512]{0:T(512)S(1)} %select_select_fusion), kind=kOutput, calls=%fused_computation.3 | convolution fusion | flops 268959744 | bytes 1050628 | tf_op jit(solution)/shard_map/dot_general | solution.py:30
  2.9 6.4 %all-to-all-start = ((bf16[8,64,512]{2,1,0:T(8,128)(2,1)}), bf16[8,64,512]{2,1,0:T(8,128)(2,1)}, u32[]{:S(2)}, u32[]{:S(2)}) async-start(bf16[8,64,512]{2,1,0:T(8,128)(2,1)} %bitcast.2), calls=%async_computation | async-start | bytes 1048576 | tf_op jit(solution)/shard_map/all_to_all | solution.py:164
  9.2 2.6 %dynamic-slice_bitcast_fusion = (bf16[1,1024,512]{2,1,0:T(8,128)(2,1)S(1)}, bf16[1024,512]{1,0:T(8,128)(2,1)}) fusion(bf16[2048,512]{1,0:T(8,128)(2,1)} %param.9, s32[]{:T(128)S(6)} %select_n.115, s32[]{:T(128)S(6)} %select_n.114), kind=kLoop, calls=%fused_computation.4 | loop fusion | bytes 4194312 | tf_op jit(solution)/shard_map/stack | solution.py:153
  11.9 1.5 %collective-permute-start = (bf16[1024,512]{1,0:T(8,128)(2,1)}, bf16[1024,512]{1,0:T(8,128)(2,1)}, u32[]{:S(2)}, u32[]{:S(2)}) collective-permute-start(bf16[1024,512]{1,0:T(8,128)(2,1)} %get-tuple-element.6), channel_id=1, source_target_pairs={{0,1},{1,0},{2,3},{3,2},{4,5},{5,4},{6,7},{7,6},{8,9},{9,8},{10,11... | collective-permute-start | bytes 3145736 | tf_op jit(solution)/shard_map/ppermute | solution.py:149
  13.3 1.5 %collective-permute-start.1 = (bf16[1024,512]{1,0:T(8,128)(2,1)}, bf16[1024,512]{1,0:T(8,128)(2,1)}, u32[]{:S(2)}, u32[]{:S(2)}) collective-permute-start(bf16[1024,512]{1,0:T(8,128)(2,1)} %get-tuple-element.6), channel_id=1, source_target_pairs={{0,2},{1,3},{2,0},{3,1},{4,6},{5,7},{6,4},{7,5},{8,10},{9,11},{10,... | collective-permute-start | bytes 3145736 | tf_op jit(solution)/shard_map/ppermute | solution.py:149
  14.9 0.5 collective-permute-start.2
  15.3 0.6 fusion.7.m_ref
  16.0 8.7 %all-to-all-done.x_ref = bf16[8,64,512]{2,1,0:T(8,128)(2,1)} async-done(((bf16[8,64,512]{2,1,0:T(8,128)(2,1)}), bf16[8,64,512]{2,1,0:T(8,128)(2,1)}, u32[]{:S(2)}, u32[]{:S(2)}) %all-to-all-start) | async-done | bytes 524320 | tf_op jit(solution)/shard_map/all_to_all | solution.py:164
  24.7 6.8 %positions.1 = f32[8,4,64,128]{3,2,1,0:T(8,128)} custom-call(bf16[8,64,512]{2,1,0:T(8,128)(2,1)} %all-to-all-done.x_ref, f32[32,1]{1,0:T(8,128)} %fusion.7.m_ref, f32[8,512]{1,0:T(8,128)} %constant.144.clone.tw_c, f32[8,512]{1,0:T(8,128)} %constant.145.clone.tw_s, bf16[512,1024]{1,0:T(8,128)(2,1)} %constant.146.clone.th_ref, ...), custom_call_target="tpu_custom_call" | custom-call | tf_op jit(solution)/shard_map/positions/pallas_call | solution.py:172
  31.4 3.7 %all-to-all-start.1 = ((f32[32,64,128]{2,1,0:T(8,128)}), f32[32,64,128]{2,1,0:T(8,128)}, u32[]{:S(2)}, u32[]{:S(2)}) async-start(f32[32,64,128]{2,1,0:T(8,128)} %bitcast.16), calls=%async_computation.1 | async-start | bytes 2097152 | tf_op jit(solution)/shard_map/all_to_all | solution.py:179
  35.1 3.1 %collective-permute-done = bf16[1024,512]{1,0:T(8,128)(2,1)} collective-permute-done((bf16[1024,512]{1,0:T(8,128)(2,1)}, bf16[1024,512]{1,0:T(8,128)(2,1)}, u32[]{:S(2)}, u32[]{:S(2)}) %collective-permute-start) | collective-permute-done | bytes 1048608 | tf_op jit(solution)/shard_map/ppermute | solution.py:149
  38.2 0.0 collective-permute-start.3
  38.2 32.7 %collective-permute-done.1 = bf16[1024,512]{1,0:T(8,128)(2,1)} collective-permute-done((bf16[1024,512]{1,0:T(8,128)(2,1)}, bf16[1024,512]{1,0:T(8,128)(2,1)}, u32[]{:S(2)}, u32[]{:S(2)}) %collective-permute-start.1) | collective-permute-done | bytes 1048608 | tf_op jit(solution)/shard_map/ppermute | solution.py:149
  70.9 0.4 collective-permute-done.2
  71.3 0.1 collective-permute-start.5
  71.4 0.6 pad_add_fusion.at_ref
  72.0 3.7 %pad_maximum_fusion.mine_ref = bf16[4,1024,512]{2,1,0:T(8,128)(2,1)} fusion(bf16[1,1024,512]{2,1,0:T(8,128)(2,1)} %bitcast.8, bf16[1,1024,512]{2,1,0:T(8,128)(2,1)} %bitcast.7, bf16[1,1024,512]{2,1,0:T(8,128)(2,1)} %bitcast.6, bf16[1,1024,512]{2,1,0:T(8,128)(2,1)} %bitcast.5), kind=kLoop, calls=%fused_computation | loop fusion | flops 6291456 | bytes 8388608 | tf_op jit(solution)/shard_map/stack | solution.py:151
  75.7 0.0 collective-permute-done.3
  75.7 2.2 %pad_maximum_fusion.1.other_ref = bf16[4,1024,512]{2,1,0:T(8,128)(2,1)} fusion(bf16[1,1024,512]{2,1,0:T(8,128)(2,1)S(1)} %bitcast.19, bf16[1,1024,512]{2,1,0:T(8,128)(2,1)S(1)} %bitcast.18, bf16[1,1024,512]{2,1,0:T(8,128)(2,1)S(1)} %bitcast.17, bf16[1,1024,512]{2,1,0:T(8,128)(2,1)S(1)} %get-tuple-element.5), kind=kLoop, calls=%fused_computation.1 | loop fusion | flops 6291456 | bytes 8388608 | tf_op jit(solution)/shard_map/stack | solution.py:153
  78.0 8.7 %outputs.1 = bf16[4,128,512]{2,1,0:T(8,128)(2,1)} custom-call(s32[2]{0:T(128)} %pad_add_fusion.at_ref, f32[8,4,64,128]{3,2,1,0:T(8,128)} %bitcast.4.z_ref, bf16[512,512]{1,0:T(8,128)(2,1)} %constant.148.clone.gh_ref, bf16[512,512]{1,0:T(8,128)(2,1)} %constant.149.clone.gl_ref, bf16[4,1024,512]{2,1,0:T(8,128)(2,1)} %pad_maximum_fusion.mine_ref, ...), custom_call_target="tpu_custom_call" | custom-call | tf_op jit(solution)/shard_map/outputs/pallas_call | solution.py:192
  86.6 3.9 %all-to-all-start.2 = ((bf16[4,128,512]{2,1,0:T(8,128)(2,1)}), bf16[4,128,512]{2,1,0:T(8,128)(2,1)S(1)}, u32[]{:S(2)}, u32[]{:S(2)}) async-start(bf16[4,128,512]{2,1,0:T(8,128)(2,1)} %outputs.1), calls=%async_computation.2 | async-start | bytes 1048576 | tf_op jit(solution)/shard_map/all_to_all | solution.py:210
  90.5 8.9 %all-to-all-done.2 = bf16[4,128,512]{2,1,0:T(8,128)(2,1)S(1)} async-done(((bf16[4,128,512]{2,1,0:T(8,128)(2,1)}), bf16[4,128,512]{2,1,0:T(8,128)(2,1)S(1)}, u32[]{:S(2)}, u32[]{:S(2)}) %all-to-all-start.2) | async-done | bytes 524320 | tf_op jit(solution)/shard_map/all_to_all | solution.py:210
  99.3 1.3 %convolution_convert_fusion = bf16[512,512]{1,0:T(8,128)(2,1)} fusion(bf16[512,512]{1,0:T(8,128)(2,1)S(1)} %bitcast.20, s32[512]{0:T(512)S(1)} %fusion.13), kind=kOutput, calls=%fused_computation.2 | convolution fusion | flops 268959744 | bytes 1050624 | tf_op jit(solution)/shard_map/dot_general | solution.py:34
  (7 shorter events, 0.0 us)
Async XLA Ops:
  0.0 1.6 %copy-start = (bf16[512,2048]{1,0:T(8,128)(2,1)S(1)}, bf16[512,2048]{1,0:T(8,128)(2,1)}, u32[]{:S(2)}) copy-start(bf16[512,2048]{1,0:T(8,128)(2,1)} %param.8) | copy-start | bytes 6291460
  2.9 21.8 %all-to-all-start = ((bf16[8,64,512]{2,1,0:T(8,128)(2,1)}), bf16[8,64,512]{2,1,0:T(8,128)(2,1)}, u32[]{:S(2)}, u32[]{:S(2)}) async-start(bf16[8,64,512]{2,1,0:T(8,128)(2,1)} %bitcast.2), calls=%async_computation | async-start | bytes 1048576 | tf_op jit(solution)/shard_map/all_to_all | solution.py:164
  11.9 26.3 %collective-permute-start = (bf16[1024,512]{1,0:T(8,128)(2,1)}, bf16[1024,512]{1,0:T(8,128)(2,1)}, u32[]{:S(2)}, u32[]{:S(2)}) collective-permute-start(bf16[1024,512]{1,0:T(8,128)(2,1)} %get-tuple-element.6), channel_id=1, source_target_pairs={{0,1},{1,0},{2,3},{3,2},{4,5},{5,4},{6,7},{7,6},{8,9},{9,8},{10,11... | collective-permute-start | bytes 3145736 | tf_op jit(solution)/shard_map/ppermute | solution.py:149
  13.3 57.5 %collective-permute-start.1 = (bf16[1024,512]{1,0:T(8,128)(2,1)}, bf16[1024,512]{1,0:T(8,128)(2,1)}, u32[]{:S(2)}, u32[]{:S(2)}) collective-permute-start(bf16[1024,512]{1,0:T(8,128)(2,1)} %get-tuple-element.6), channel_id=1, source_target_pairs={{0,2},{1,3},{2,0},{3,1},{4,6},{5,7},{6,4},{7,5},{8,10},{9,11},{10,... | collective-permute-start | bytes 3145736 | tf_op jit(solution)/shard_map/ppermute | solution.py:149
  14.9 56.4 %collective-permute-start.2 = (bf16[1024,512]{1,0:T(8,128)(2,1)}, bf16[1024,512]{1,0:T(8,128)(2,1)}, u32[]{:S(2)}, u32[]{:S(2)}) collective-permute-start(bf16[1024,512]{1,0:T(8,128)(2,1)} %get-tuple-element.6), channel_id=1, source_target_pairs={{0,3},{1,2},{2,1},{3,0},{4,7},{5,6},{6,5},{7,4},{8,11},{9,10},{10,... | collective-permute-start | bytes 3145736 | tf_op jit(solution)/shard_map/ppermute | solution.py:149
  31.4 46.5 %all-to-all-start.1 = ((f32[32,64,128]{2,1,0:T(8,128)}), f32[32,64,128]{2,1,0:T(8,128)}, u32[]{:S(2)}, u32[]{:S(2)}) async-start(f32[32,64,128]{2,1,0:T(8,128)} %bitcast.16), calls=%async_computation.1 | async-start | bytes 2097152 | tf_op jit(solution)/shard_map/all_to_all | solution.py:179
  38.2 37.5 %collective-permute-start.3 = (bf16[1024,512]{1,0:T(8,128)(2,1)}, bf16[1024,512]{1,0:T(8,128)(2,1)S(1)}, u32[]{:S(2)}, u32[]{:S(2)}) collective-permute-start(bf16[1024,512]{1,0:T(8,128)(2,1)} %collective-permute-done), channel_id=1, source_target_pairs={{0,4},{4,0},{8,12},{12,8},{16,20},{20,16},{24,28},{28,24},{1,5},{5... | collective-permute-start | bytes 3145736 | tf_op jit(solution)/shard_map/ppermute | solution.py:152
  70.9 4.8 %collective-permute-start.4 = (bf16[1024,512]{1,0:T(8,128)(2,1)}, bf16[1024,512]{1,0:T(8,128)(2,1)S(1)}, u32[]{:S(2)}, u32[]{:S(2)}) collective-permute-start(bf16[1024,512]{1,0:T(8,128)(2,1)} %collective-permute-done.1), channel_id=1, source_target_pairs={{0,4},{4,0},{8,12},{12,8},{16,20},{20,16},{24,28},{28,24},{1,5},{5... | collective-permute-start | bytes 3145736 | tf_op jit(solution)/shard_map/ppermute | solution.py:152
  71.3 4.4 %collective-permute-start.5 = (bf16[1024,512]{1,0:T(8,128)(2,1)}, bf16[1024,512]{1,0:T(8,128)(2,1)S(1)}, u32[]{:S(2)}, u32[]{:S(2)}) collective-permute-start(bf16[1024,512]{1,0:T(8,128)(2,1)} %collective-permute-done.2), channel_id=1, source_target_pairs={{0,4},{4,0},{8,12},{12,8},{16,20},{20,16},{24,28},{28,24},{1,5},{5... | collective-permute-start | bytes 3145736 | tf_op jit(solution)/shard_map/ppermute | solution.py:152
  86.6 12.7 %all-to-all-start.2 = ((bf16[4,128,512]{2,1,0:T(8,128)(2,1)}), bf16[4,128,512]{2,1,0:T(8,128)(2,1)S(1)}, u32[]{:S(2)}, u32[]{:S(2)}) async-start(bf16[4,128,512]{2,1,0:T(8,128)(2,1)} %outputs.1), calls=%async_computation.2 | async-start | bytes 1048576 | tf_op jit(solution)/shard_map/all_to_all | solution.py:210
where the time goes:
time: 101 us
  waiting for transfers between devices  53.7 us (53%)
  starting transfers between devices  17.5 us (17%)
  Pallas kernels  15.4 us (15%)
  other arithmetic  7.17 us (7%)
  local copies, waits for them, and re-layouts  4.21 us (4%)
  matrix products  2.55 us (3%)
    ppermute x3, waiting for transfers between devices, body(): lax.ppermute(own, 'col', [(c, c ^ d) for c in range(cols)])  36.2 us
    all_to_all x1, waiting for transfers between devices, body(): lax.all_to_all(out, 'col', split_axis=0, concat_axis=0, tiled=True)  8.86 us
    all_to_all x1, waiting for transfers between devices, body(): lax.all_to_all(turned, 'row', split_axis=0, concat_axis=0, tiled=True)  8.69 us
    pallas_call x1, Pallas kernels, body(): pl.pallas_call(output_kernel, out_shape=jax.ShapeDtypeStruct((cols, few,...  8.65 us
    pallas_call x1, Pallas kernels, body(): pl.pallas_call(position_kernel, out_shape=jax.ShapeDtypeStruct((rows, col...  6.79 us
    all_to_all x1, starting transfers between devices, body(): lax.all_to_all(turned, 'row', split_axis=0, concat_axis=0, tiled=True)  6.35 us
    all_to_all x1, starting transfers between devices, body(): lax.all_to_all(out, 'col', split_axis=0, concat_axis=0, tiled=True)  3.86 us
    another operation x1, other arithmetic, body(): mine = jnp.stack([own] + fetched)  3.71 us
  transfers between devices with their start and end apart: 9, of which 5 were waited for; matrix products, arithmetic and copies ran while one was open for 10% of the time, Pallas kernels for 7%

commit v1 on v0

v1 whole, which is shorter than its diff:
```python
import math

import jax
import jax.numpy as jnp
import numpy as np
from jax import lax
from jax.experimental import pallas as pl
from jax.experimental.pallas import tpu as pltpu
from jax.sharding import PartitionSpec as P


GROUPS = 4
GROUP_DIM = 512
HALF = GROUP_DIM // 2
BF = jnp.bfloat16
F32 = jnp.float32


def two_parts(table):
    high = np.asarray(table, np.float32).astype(BF)
    low = (np.asarray(table, np.float64) - high.astype(np.float64)).astype(np.float32).astype(BF)
    return high, low


def split(value):
    high = value.astype(BF)
    return high, (value - high.astype(F32)).astype(BF)


def dot_nt(left, right):
    return lax.dot_general(left, right, (((1,), (1,)), ((), ())), preferred_element_type=F32)


def dot_nn(left, right):
    return jnp.dot(left, right, preferred_element_type=F32)


def plus(left, right, sign=1):
    if right is None:
        return left
    if left is None:
        return right if sign > 0 else -right
    return left + right if sign > 0 else left - right


def times(weight, value):
    if value is None or abs(weight) < 1e-9:
        return None
    if abs(weight - 1.0) < 1e-9:
        return value
    return -value if abs(weight + 1.0) < 1e-9 else weight * value


def real_dft(values):
    n = len(values)
    if n == 1:
        return [(values[0], None)]
    even, odd = real_dft(values[::2]), real_dft(values[1::2])
    terms = [None] * (n // 2 + 1)
    for k in range(n // 4 + 1):
        c, s = math.cos(2 * math.pi * k / n), -math.sin(2 * math.pi * k / n)
        re = plus(times(c, odd[k][0]), times(s, odd[k][1]), -1)
        im = plus(times(c, odd[k][1]), times(s, odd[k][0]))
        terms[n // 2 - k] = (plus(even[k][0], re, -1), times(-1.0, plus(even[k][1], im, -1)))
        terms[k] = (plus(even[k][0], re), plus(even[k][1], im))
    return terms


def position_kernel(x_ref, m_ref, tw_c, tw_s, th_ref, tl_ref, o_ref, lh_ref, ll_ref):
    rows, chans, seg = x_ref.shape
    pairs = chans // 2
    cols = o_ref.shape[1]
    kb = o_ref.shape[2]
    mask = m_ref[...]
    evens, odds = [], []
    for r in range(rows):
        block = x_ref[r].astype(F32)
        lo, hi = block[:pairs], block[pairs:]
        evens.append(lo + mask * hi)
        odds.append(mask * lo + (1.0 - 2.0 * mask) * hi)

    def place(at, left, right):
        for side, value in ((0, left), (seg, right)):
            high, low = split(value)
            lh_ref[at : at + pairs, side : side + seg] = high
            ll_ref[at : at + pairs, side : side + seg] = low

    zero = jnp.zeros((pairs, seg), F32)
    even_terms, odd_terms = real_dft(evens), real_dft(odds)
    for j0 in range(rows // 2 + 1):
        er, ei = (zero if v is None else v for v in even_terms[j0])
        orr, oi = (zero if v is None else v for v in odd_terms[j0])
        for j, sign in ((j0, 1.0), (rows - j0, -1.0)):
            if j == rows or (sign < 0 and j == j0):
                continue
            c, s = tw_c[j : j + 1], tw_s[j : j + 1]
            ein, oin = sign * ei, sign * oi
            place(j * chans, er * c + ein * s, ein * c - er * s)
            tr, ti = orr * c + oin * s, oin * c - orr * s
            place(
                j * chans + pairs,
                (1.0 - mask) * tr - mask * ti,
                mask * tr + (1.0 - mask) * ti,
            )
    width = o_ref.shape[3]
    for c in range(cols):
        lh, ll = lh_ref[c * width : (c + 1) * width], ll_ref[c * width : (c + 1) * width]
        th = th_ref[...]
        z = dot_nt(th, lh) + dot_nt(th, ll) + dot_nt(tl_ref[...], lh)
        for r in range(rows):
            o_ref[r, c] = z[r * kb : (r + 1) * kb]


def output_kernel(at_ref, z_ref, gh_ref, gl_ref, own_ref, *refs):
    rows, cols, kb, width = z_ref.shape
    total = own_ref.shape[0]
    mine, other = refs[: cols - 1], refs[cols - 1 : 2 * (cols - 1)]
    o_ref, zh_ref, zl_ref, sh_ref, own_v, mine_v, other_v, sems = refs[2 * (cols - 1) :]
    chans = total // (rows * cols)
    jb = width // chans
    own_copy = pltpu.make_async_copy(own_ref, own_v, sems.at[0])
    own_copy.start()
    copies = []
    for d in range(cols - 1):
        pair = (
            pltpu.make_async_copy(mine[d], mine_v.at[d], sems.at[1 + 2 * d]),
            pltpu.make_async_copy(other[d], other_v.at[d], sems.at[2 + 2 * d]),
        )
        for copy in pair:
            copy.start()
        copies.append(pair)

    for c in range(cols):
        for r in range(rows):
            high, low = split(z_ref[r, c])
            lane = (c * rows + r) * chans
            for jj in range(jb):
                zh_ref[jj * kb : (jj + 1) * kb, lane : lane + chans] = high[:, jj * chans : (jj + 1) * chans]
                zl_ref[jj * kb : (jj + 1) * kb, lane : lane + chans] = low[:, jj * chans : (jj + 1) * chans]
    few = jb * kb
    for g in range(GROUPS):
        cut = slice(g * GROUP_DIM, (g + 1) * GROUP_DIM)
        zh, zl = zh_ref[:, cut], zl_ref[:, cut]
        gh = gh_ref[...]
        spectral = dot_nn(zh, gh) + dot_nn(zl, gh) + dot_nn(zh, gl_ref[...])
        high, low = split(spectral)
        half, at = divmod(g * GROUP_DIM, total // 2)
        sh_ref[half, :few, at : at + GROUP_DIM] = high
        sh_ref[half, few:, at : at + GROUP_DIM] = low

    half, col = at_ref[0], at_ref[1]
    own_copy.wait()
    both = dot_nn(sh_ref[0], own_v[: total // 2]) + dot_nn(sh_ref[1], own_v[total // 2 :])
    o_ref[col] = (both[:few] + both[few:]).astype(BF)
    for d in range(cols - 1):
        for copy in copies[d]:
            copy.wait()
        both = dot_nn(sh_ref[half], mine_v[d]) + dot_nn(sh_ref[1 - half], other_v[d])
        o_ref[jnp.bitwise_xor(col, d + 1)] = (both[:few] + both[few:]).astype(BF)


def body(tokens, out_weight):
    seg, dim = tokens.shape
    out_cols = out_weight.shape[1]
    rows = lax.axis_size("row")
    cols = lax.axis_size("col")
    row, col = lax.axis_index("row"), lax.axis_index("col")
    length = seg * rows
    chans = dim // (rows * cols)
    pairs = chans // 2
    jb, kb = rows // cols, seg // rows

    half = row % 2
    own = lax.dynamic_slice(out_weight, (half * (dim // 2), 0), (dim // 2, out_cols))
    fetched, swapped = [], []
    for d in range(1, cols):
        fetched.append(lax.ppermute(own, "col", [(c, c ^ d) for c in range(cols)]))
        swapped.append(lax.ppermute(fetched[-1], "row", [(r, r ^ 1) for r in range(rows)]))

    group = (col * GROUPS) // cols
    group_tokens = lax.dynamic_slice(tokens, (0, group * GROUP_DIM), (seg, GROUP_DIM))
    slot = jnp.arange(rows * chans, dtype=jnp.int32)
    pair = (col * rows + slot // chans) * pairs + (slot % chans) % pairs
    p = pair % HALF
    upper = (slot % chans) >= pairs
    channel = jnp.where(upper, jnp.where(p == 0, HALF, GROUP_DIM - p), p)
    pick = (channel[:, None] == jnp.arange(GROUP_DIM, dtype=jnp.int32)[None, :]).astype(BF)
    turned = dot_nt(pick, group_tokens).astype(BF).reshape(rows, chans, seg)
    whole = lax.all_to_all(turned, "row", split_axis=0, concat_axis=0, tiled=True)

    own_pair = (col * rows + row) * pairs + jnp.arange(pairs, dtype=jnp.int32)
    mask = ((own_pair % HALF) != 0).astype(F32)[:, None]
    s_at = np.arange(seg)
    twist = 2 * np.pi * ((np.arange(rows)[:, None] * s_at[None, :]) % length) / length
    phase = 2 * np.pi * ((s_at[:, None] * s_at[None, :]) % seg) / seg
    th, tl = two_parts(np.concatenate([np.cos(phase), np.sin(phase)], axis=1))
    in_vmem = pl.BlockSpec(memory_space=pltpu.VMEM)
    spread = pl.pallas_call(
        position_kernel,
        out_shape=jax.ShapeDtypeStruct((rows, cols, kb, jb * chans), F32),
        in_specs=[in_vmem] * 6,
        scratch_shapes=[pltpu.VMEM((rows * chans, 2 * seg), BF)] * 2,
        compiler_params=pltpu.CompilerParams(vmem_limit_bytes=20 * 1024 * 1024),
        name="positions",
    )(whole, mask, np.cos(twist).astype(np.float32), np.sin(twist).astype(np.float32), th, tl)
    flat = spread.reshape(rows * cols, kb, jb * chans)
    mixed_in = lax.all_to_all(flat, ("row", "col"), split_axis=0, concat_axis=0, tiled=True)
    mixed_in = mixed_in.reshape(rows, cols, kb, jb * chans)

    lanes = np.arange(GROUP_DIM)
    lp = (lanes // chans) * pairs + (lanes % chans) % pairs
    odd = (lanes % chans) >= pairs
    turn = 2 * np.pi * ((lp[:, None] * lanes[None, :]) % GROUP_DIM) / GROUP_DIM
    flip = np.where(lanes % 2 == 0, 1.0, -1.0)[None, :]
    grid_table = np.where(odd[:, None], np.where(lp[:, None] == 0, flip, -np.sin(turn)), np.cos(turn))
    gh, gl = two_parts(grid_table / math.sqrt(length * GROUP_DIM))
    places = jnp.stack([half, col]).astype(jnp.int32)
    few = jb * kb
    anywhere = pl.BlockSpec(memory_space=pl.ANY)
    out = pl.pallas_call(
        output_kernel,
        out_shape=jax.ShapeDtypeStruct((cols, few, out_cols), BF),
        in_specs=[pl.BlockSpec(memory_space=pltpu.SMEM), in_vmem, in_vmem, in_vmem]
        + [anywhere] * (2 * cols - 1),
        scratch_shapes=[pltpu.VMEM((few, dim), BF)] * 2
        + [
            pltpu.VMEM((2, 2 * few, dim // 2), BF),
            pltpu.VMEM((dim, out_cols), BF),
            pltpu.VMEM((cols - 1, dim // 2, out_cols), BF),
            pltpu.VMEM((cols - 1, dim // 2, out_cols), BF),
            pltpu.SemaphoreType.DMA((2 * cols - 1,)),
        ],
        compiler_params=pltpu.CompilerParams(vmem_limit_bytes=26 * 1024 * 1024),
        name="outputs",
    )(places, mixed_in, gh, gl, out_weight, *fetched, *swapped)
    gathered = lax.all_to_all(out, "col", split_axis=0, concat_axis=0, tiled=True)
    gathered = gathered.reshape(seg, out_cols)
    at = jnp.arange(seg, dtype=jnp.int32)
    wanted = (at % rows) * kb + at // rows
    order = (wanted[:, None] == at[None, :]).astype(BF)
    return dot_nn(order, gathered).astype(BF)


def solution(mesh):
    placed = (P("row", None), P(None, "col"))
    return jax.shard_map(
        body, mesh=mesh, in_specs=placed, out_specs=P("row", "col"), check_vma=False
    )
```

time: 101 us -> 104 us (1.030)
  local copies, waits for them, and re-layouts: 4.21 us -> 17.4 us
  other arithmetic: 7.17 us -> 0.11 us
  Pallas kernels: 15.4 us -> 9.82 us
  waiting for transfers between devices: 53.7 us -> 55.9 us
    unnamed x2 -> x30, local copies, waits for them, and re-layouts: 1.57 us -> 15.1 us
    another operation x2 -> x0, other arithmetic: 5.96 us -> none  [the longest x1 3.71 us: body(): mine = jnp.stack([own] + fetched)]
    pallas_call x1, Pallas kernels: 8.65 us -> 5.01 us  [body(): pl.pallas_call(output_kernel, out_shape=jax.ShapeDtypeStruct((cols, few,...]
    another operation x1 -> x0, local copies, waits for them, and re-layouts: 2.64 us -> none  [body(): other = jnp.stack([rest] + swapped)]
    dynamic_slice x0 -> x1, local copies, waits for them, and re-layouts: none -> 2.3 us  [body(): lax.dynamic_slice(out_weight, (half * (dim // 2), 0), (dim // 2, out_cols))]
    pallas_call x1, Pallas kernels: 6.79 us -> 4.8 us  [body(): pl.pallas_call(position_kernel, out_shape=jax.ShapeDtypeStruct((rows, col...]
    ppermute x6, waiting for transfers between devices: 36.2 us -> 37.4 us  [the longest x3 35.6 us: body(): fetched.append(lax.ppermute(own, 'col', [(c, c ^ d) for c in range(cols)]))]
  transfers between devices with their start and end apart: 9 -> 9, of which waited for: 5 -> 7; matrix products, arithmetic and copies ran while one was open for 10% -> 2% of each run, Pallas kernels for 7% -> 5%
where the time goes in v1:
time: 104 us; the launch traced here: 103 us
  waiting for transfers between devices  55.9 us (54%)
  local copies, waits for them, and re-layouts  17.4 us (17%)
  starting transfers between devices  17.3 us (17%)
  Pallas kernels  9.82 us (9%)
  matrix products  2.55 us (2%)
    ppermute x3, waiting for transfers between devices, body(): fetched.append(lax.ppermute(own, 'col', [(c, c ^ d) for c in range(cols)]))  35.6 us
    unnamed x30, local copies, waits for them, and re-layouts  15.1 us
    all_to_all x1, waiting for transfers between devices, body(): lax.all_to_all(turned, 'row', split_axis=0, concat_axis=0, tiled=True)  9.52 us
    all_to_all x1, waiting for transfers between devices, body(): lax.all_to_all(out, 'col', split_axis=0, concat_axis=0, tiled=True)  9 us
    all_to_all x1, starting transfers between devices, body(): lax.all_to_all(turned, 'row', split_axis=0, concat_axis=0, tiled=True)  6.35 us
    pallas_call x1, Pallas kernels, body(): pl.pallas_call(output_kernel, out_shape=jax.ShapeDtypeStruct((cols, few,...  5.01 us
    pallas_call x1, Pallas kernels, body(): pl.pallas_call(position_kernel, out_shape=jax.ShapeDtypeStruct((rows, col...  4.8 us
    all_to_all x1, starting transfers between devices, body(): lax.all_to_all(out, 'col', split_axis=0, concat_axis=0, tiled=True)  3.85 us
  transfers between devices with their start and end apart: 9, of which 7 were waited for; matrix products, arithmetic and copies ran while one was open for 2% of the time, Pallas kernels for 5%

profile of v1, /device:TPU:0, one launch (start us, length us, event | category | flops | bytes accessed | tf_op | source)
XLA Modules:
  0.0 103.2 jit_solution(10954487278196652960)
XLA Ops:
  0.0 1.6 %copy-done = bf16[512,2048]{1,0:T(8,128)(2,1)S(1)} copy-done((bf16[512,2048]{1,0:T(8,128)(2,1)S(1)}, bf16[512,2048]{1,0:T(8,128)(2,1)}, u32[]{:S(2)}) %copy-start) | copy-done | bytes 2097176
  1.6 1.3 %convolution_convert_fusion.1 = bf16[512,512]{1,0:T(8,128)(2,1)} fusion(bf16[512,2048]{1,0:T(8,128)(2,1)S(1)} %copy-done, s32[]{:T(128)S(6)} %select_n.109, s32[512]{0:T(512)S(1)} %select_select_fusion), kind=kOutput, calls=%fused_computation.1 | convolution fusion | flops 268959744 | bytes 1050628 | tf_op jit(solution)/shard_map/dot_general | solution.py:31
  2.9 6.4 %all-to-all-start = ((bf16[8,64,512]{2,1,0:T(8,128)(2,1)}), bf16[8,64,512]{2,1,0:T(8,128)(2,1)S(1)}, u32[]{:S(2)}, u32[]{:S(2)}) async-start(bf16[8,64,512]{2,1,0:T(8,128)(2,1)} %bitcast.2), calls=%async_computation | async-start | bytes 1048576 | tf_op jit(solution)/shard_map/all_to_all | solution.py:189
  9.2 2.3 %constant_dynamic-slice_fusion = bf16[1024,512]{1,0:T(8,128)(2,1)} fusion(bf16[2048,512]{1,0:T(8,128)(2,1)} %own_ref.1, s32[]{:T(128)S(6)} %select_n.111), kind=kLoop, calls=%fused_computation.48 | loop fusion | bytes 2097156 | tf_op jit(solution)/shard_map/dynamic_slice | solution.py:174
  11.5 1.5 %collective-permute-start = (bf16[1024,512]{1,0:T(8,128)(2,1)}, bf16[1024,512]{1,0:T(8,128)(2,1)}, u32[]{:S(2)}, u32[]{:S(2)}) collective-permute-start(bf16[1024,512]{1,0:T(8,128)(2,1)} %constant_dynamic-slice_fusion), channel_id=1, source_target_pairs={{0,1},{1,0},{2,3},{3,2},{4,5},{5,4},{6,7},{7,6},{8,9},{9,8},{10,11... | collective-permute-start | bytes 3145736 | tf_op jit(solution)/shard_map/ppermute | solution.py:177
  13.0 1.5 %collective-permute-start.1 = (bf16[1024,512]{1,0:T(8,128)(2,1)}, bf16[1024,512]{1,0:T(8,128)(2,1)}, u32[]{:S(2)}, u32[]{:S(2)}) collective-permute-start(bf16[1024,512]{1,0:T(8,128)(2,1)} %constant_dynamic-slice_fusion), channel_id=1, source_target_pairs={{0,2},{1,3},{2,0},{3,1},{4,6},{5,7},{6,4},{7,5},{8,10},{9,11},{10,... | collective-permute-start | bytes 3145736 | tf_op jit(solution)/shard_map/ppermute | solution.py:177
  15.0 9.5 %all-to-all-done.x_ref = bf16[8,64,512]{2,1,0:T(8,128)(2,1)S(1)} async-done(((bf16[8,64,512]{2,1,0:T(8,128)(2,1)}), bf16[8,64,512]{2,1,0:T(8,128)(2,1)S(1)}, u32[]{:S(2)}, u32[]{:S(2)}) %all-to-all-start) | async-done | bytes 524320 | tf_op jit(solution)/shard_map/all_to_all | solution.py:189
  24.6 1.2 %copy-done.3 = bf16[512,1024]{1,0:T(8,128)(2,1)S(1)} copy-done((bf16[512,1024]{1,0:T(8,128)(2,1)S(1)}, bf16[512,1024]{1,0:T(8,128)(2,1)}, u32[]{:S(2)}) %copy-start.3) | copy-done | bytes 1048600
  25.8 1.2 %copy-done.4 = bf16[512,1024]{1,0:T(8,128)(2,1)S(1)} copy-done((bf16[512,1024]{1,0:T(8,128)(2,1)S(1)}, bf16[512,1024]{1,0:T(8,128)(2,1)}, u32[]{:S(2)}) %copy-start.4) | copy-done | bytes 1048600
  27.0 4.8 %positions.1 = f32[8,4,64,128]{3,2,1,0:T(8,128)} custom-call(bf16[8,64,512]{2,1,0:T(8,128)(2,1)S(1)} %all-to-all-done.x_ref, f32[32,1]{1,0:T(8,128)S(1)} %fusion.7.m_ref, f32[8,512]{1,0:T(8,128)S(1)} %copy-done.13, f32[8,512]{1,0:T(8,128)S(1)} %copy-done.14, bf16[512,1024]{1,0:T(8,128)(2,1)S(1)} %copy-done.3, bf16[512,1024]{1,0:T(8,128)(2,1)S(1)} %copy-done.4), custom_call_target="tpu_custom_call" | custom-call | tf_op jit(solution)/shard_map/positions/pallas_call | solution.py:198
  31.8 3.5 %all-to-all-start.1 = ((f32[32,64,128]{2,1,0:T(8,128)}), f32[32,64,128]{2,1,0:T(8,128)S(1)}, u32[]{:S(2)}, u32[]{:S(2)}) async-start(f32[32,64,128]{2,1,0:T(8,128)} %bitcast.3), calls=%async_computation.1 | async-start | bytes 2097152 | tf_op jit(solution)/shard_map/all_to_all | solution.py:207
  35.4 2.5 %collective-permute-done.refs_0_ = bf16[1024,512]{1,0:T(8,128)(2,1)} collective-permute-done((bf16[1024,512]{1,0:T(8,128)(2,1)}, bf16[1024,512]{1,0:T(8,128)(2,1)}, u32[]{:S(2)}, u32[]{:S(2)}) %collective-permute-start) | collective-permute-done | bytes 1048608 | tf_op jit(solution)/shard_map/ppermute | solution.py:177
  37.9 32.7 %collective-permute-done.1.refs_1_ = bf16[1024,512]{1,0:T(8,128)(2,1)} collective-permute-done((bf16[1024,512]{1,0:T(8,128)(2,1)}, bf16[1024,512]{1,0:T(8,128)(2,1)}, u32[]{:S(2)}, u32[]{:S(2)}) %collective-permute-start.1) | collective-permute-done | bytes 1048608 | tf_op jit(solution)/shard_map/ppermute | solution.py:177
  72.2 1.3 %collective-permute-done.4.refs_4_ = bf16[1024,512]{1,0:T(8,128)(2,1)S(1)} collective-permute-done((bf16[1024,512]{1,0:T(8,128)(2,1)}, bf16[1024,512]{1,0:T(8,128)(2,1)S(1)}, u32[]{:S(2)}, u32[]{:S(2)}) %collective-permute-start.4) | collective-permute-done | bytes 1048608 | tf_op jit(solution)/shard_map/ppermute | solution.py:178
  75.9 1.6 %copy-done.1 = bf16[2048,512]{1,0:T(8,128)(2,1)S(1)} copy-done((bf16[2048,512]{1,0:T(8,128)(2,1)S(1)}, bf16[2048,512]{1,0:T(8,128)(2,1)}, u32[]{:S(2)}) %copy-start.1) | copy-done | bytes 2097176
  77.5 1.2 %copy-done.6 = bf16[1024,512]{1,0:T(8,128)(2,1)S(1)} copy-done((bf16[1024,512]{1,0:T(8,128)(2,1)S(1)}, bf16[1024,512]{1,0:T(8,128)(2,1)}, u32[]{:S(2)}) %copy-start.6) | copy-done | bytes 1048600
  78.7 1.2 %copy-done.8 = bf16[1024,512]{1,0:T(8,128)(2,1)S(1)} copy-done((bf16[1024,512]{1,0:T(8,128)(2,1)S(1)}, bf16[1024,512]{1,0:T(8,128)(2,1)}, u32[]{:S(2)}) %copy-start.8) | copy-done | bytes 1048600
  79.9 1.2 %copy-done.10 = bf16[1024,512]{1,0:T(8,128)(2,1)S(1)} copy-done((bf16[1024,512]{1,0:T(8,128)(2,1)S(1)}, bf16[1024,512]{1,0:T(8,128)(2,1)}, u32[]{:S(2)}) %copy-start.10) | copy-done | bytes 1048600
  81.2 1.0 %copy-done.11 = bf16[512,512]{1,0:T(8,128)(2,1)S(1)} copy-done((bf16[512,512]{1,0:T(8,128)(2,1)S(1)}, bf16[512,512]{1,0:T(8,128)(2,1)}, u32[]{:S(2)}) %copy-start.11) | copy-done | bytes 524312
  82.2 1.0 %copy-done.12 = bf16[512,512]{1,0:T(8,128)(2,1)S(1)} copy-done((bf16[512,512]{1,0:T(8,128)(2,1)S(1)}, bf16[512,512]{1,0:T(8,128)(2,1)}, u32[]{:S(2)}) %copy-start.12) | copy-done | bytes 524312
  83.2 5.0 %outputs.1 = bf16[4,128,512]{2,1,0:T(8,128)(2,1)S(1)} custom-call(s32[2]{0:T(128)S(1)} %pad_add_fusion.at_ref, f32[8,4,64,128]{3,2,1,0:T(8,128)S(1)} %bitcast.7, bf16[512,512]{1,0:T(8,128)(2,1)S(1)} %copy-done.11, bf16[512,512]{1,0:T(8,128)(2,1)S(1)} %copy-done.12, bf16[2048,512]{1,0:T(8,128)(2,1)S(1)} %copy-done.1, ...), custom_call_target="tpu_custom_call" | custom-call | tf_op jit(solution)/shard_map/outputs/pallas_call | solution.py:220
  89.1 3.9 %all-to-all-start.2 = ((bf16[4,128,512]{2,1,0:T(8,128)(2,1)}), bf16[4,128,512]{2,1,0:T(8,128)(2,1)S(1)}, u32[]{:S(2)}, u32[]{:S(2)}) async-start(bf16[4,128,512]{2,1,0:T(8,128)(2,1)} %copy-done.2), calls=%async_computation.2 | async-start | bytes 1048576 | tf_op jit(solution)/shard_map/all_to_all | solution.py:236
  92.9 9.0 %all-to-all-done.2 = bf16[4,128,512]{2,1,0:T(8,128)(2,1)S(1)} async-done(((bf16[4,128,512]{2,1,0:T(8,128)(2,1)}), bf16[4,128,512]{2,1,0:T(8,128)(2,1)S(1)}, u32[]{:S(2)}, u32[]{:S(2)}) %all-to-all-start.2) | async-done | bytes 524320 | tf_op jit(solution)/shard_map/all_to_all | solution.py:236
  101.9 1.3 %convolution_convert_fusion = bf16[512,512]{1,0:T(8,128)(2,1)} fusion(bf16[512,512]{1,0:T(8,128)(2,1)S(1)} %bitcast.8, s32[512]{0:T(512)S(1)} %fusion.13), kind=kOutput, calls=%fused_computation | convolution fusion | flops 268959744 | bytes 1050624 | tf_op jit(solution)/shard_map/dot_general | solution.py:35
  (33 shorter events, 5.4 us)
Async XLA Ops:
  0.0 1.6 %copy-start = (bf16[512,2048]{1,0:T(8,128)(2,1)S(1)}, bf16[512,2048]{1,0:T(8,128)(2,1)}, u32[]{:S(2)}) copy-start(bf16[512,2048]{1,0:T(8,128)(2,1)} %param.8) | copy-start | bytes 6291460
  1.6 23.0 %copy-start.13 = (f32[8,512]{1,0:T(8,128)S(1)}, f32[8,512]{1,0:T(8,128)}, u32[]{:S(2)}) copy-start(f32[8,512]{1,0:T(8,128)} %constant.143.clone.tw_c) | copy-start | bytes 49156
  1.6 23.0 %copy-start.14 = (f32[8,512]{1,0:T(8,128)S(1)}, f32[8,512]{1,0:T(8,128)}, u32[]{:S(2)}) copy-start(f32[8,512]{1,0:T(8,128)} %constant.144.clone.tw_s) | copy-start | bytes 49156
  2.9 21.7 %all-to-all-start = ((bf16[8,64,512]{2,1,0:T(8,128)(2,1)}), bf16[8,64,512]{2,1,0:T(8,128)(2,1)S(1)}, u32[]{:S(2)}, u32[]{:S(2)}) async-start(bf16[8,64,512]{2,1,0:T(8,128)(2,1)} %bitcast.2), calls=%async_computation | async-start | bytes 1048576 | tf_op jit(solution)/shard_map/all_to_all | solution.py:189
  11.5 26.3 %collective-permute-start = (bf16[1024,512]{1,0:T(8,128)(2,1)}, bf16[1024,512]{1,0:T(8,128)(2,1)}, u32[]{:S(2)}, u32[]{:S(2)}) collective-permute-start(bf16[1024,512]{1,0:T(8,128)(2,1)} %constant_dynamic-slice_fusion), channel_id=1, source_target_pairs={{0,1},{1,0},{2,3},{3,2},{4,5},{5,4},{6,7},{7,6},{8,9},{9,8},{10,11... | collective-permute-start | bytes 3145736 | tf_op jit(solution)/shard_map/ppermute | solution.py:177
  13.0 57.5 %collective-permute-start.1 = (bf16[1024,512]{1,0:T(8,128)(2,1)}, bf16[1024,512]{1,0:T(8,128)(2,1)}, u32[]{:S(2)}, u32[]{:S(2)}) collective-permute-start(bf16[1024,512]{1,0:T(8,128)(2,1)} %constant_dynamic-slice_fusion), channel_id=1, source_target_pairs={{0,2},{1,3},{2,0},{3,1},{4,6},{5,7},{6,4},{7,5},{8,10},{9,11},{10,... | collective-permute-start | bytes 3145736 | tf_op jit(solution)/shard_map/ppermute | solution.py:177
  14.5 56.5 %collective-permute-start.2 = (bf16[1024,512]{1,0:T(8,128)(2,1)}, bf16[1024,512]{1,0:T(8,128)(2,1)}, u32[]{:S(2)}, u32[]{:S(2)}) collective-permute-start(bf16[1024,512]{1,0:T(8,128)(2,1)} %constant_dynamic-slice_fusion), channel_id=1, source_target_pairs={{0,3},{1,2},{2,1},{3,0},{4,7},{5,6},{6,5},{7,4},{8,11},{9,10},{10,... | collective-permute-start | bytes 3145736 | tf_op jit(solution)/shard_map/ppermute | solution.py:177
  24.6 1.2 %copy-start.3 = (bf16[512,1024]{1,0:T(8,128)(2,1)S(1)}, bf16[512,1024]{1,0:T(8,128)(2,1)}, u32[]{:S(2)}) copy-start(bf16[512,1024]{1,0:T(8,128)(2,1)} %constant.145.clone.th_ref) | copy-start | bytes 3145732
  25.8 1.2 %copy-start.4 = (bf16[512,1024]{1,0:T(8,128)(2,1)S(1)}, bf16[512,1024]{1,0:T(8,128)(2,1)}, u32[]{:S(2)}) copy-start(bf16[512,1024]{1,0:T(8,128)(2,1)} %constant.146.clone.tl_ref) | copy-start | bytes 3145732
  31.8 44.1 %all-to-all-start.1 = ((f32[32,64,128]{2,1,0:T(8,128)}), f32[32,64,128]{2,1,0:T(8,128)S(1)}, u32[]{:S(2)}, u32[]{:S(2)}) async-start(f32[32,64,128]{2,1,0:T(8,128)} %bitcast.3), calls=%async_computation.1 | async-start | bytes 2097152 | tf_op jit(solution)/shard_map/all_to_all | solution.py:207
  37.9 33.3 %collective-permute-start.3 = (bf16[1024,512]{1,0:T(8,128)(2,1)}, bf16[1024,512]{1,0:T(8,128)(2,1)S(1)}, u32[]{:S(2)}, u32[]{:S(2)}) collective-permute-start(bf16[1024,512]{1,0:T(8,128)(2,1)} %collective-permute-done.refs_0_), channel_id=1, source_target_pairs={{0,4},{4,0},{8,12},{12,8},{16,20},{20,16},{24,28},{28,24},{1,5},{5... | collective-permute-start | bytes 3145736 | tf_op jit(solution)/shard_map/ppermute | solution.py:178
  70.6 2.9 %collective-permute-start.4 = (bf16[1024,512]{1,0:T(8,128)(2,1)}, bf16[1024,512]{1,0:T(8,128)(2,1)S(1)}, u32[]{:S(2)}, u32[]{:S(2)}) collective-permute-start(bf16[1024,512]{1,0:T(8,128)(2,1)} %collective-permute-done.1.refs_1_), channel_id=1, source_target_pairs={{0,4},{4,0},{8,12},{12,8},{16,20},{20,16},{24,28},{28,24},{1,5},{5... | collective-permute-start | bytes 3145736 | tf_op jit(solution)/shard_map/ppermute | solution.py:178
  71.0 3.9 %collective-permute-start.5 = (bf16[1024,512]{1,0:T(8,128)(2,1)}, bf16[1024,512]{1,0:T(8,128)(2,1)S(1)}, u32[]{:S(2)}, u32[]{:S(2)}) collective-permute-start(bf16[1024,512]{1,0:T(8,128)(2,1)} %collective-permute-done.2.refs_2_), channel_id=1, source_target_pairs={{0,4},{4,0},{8,12},{12,8},{16,20},{20,16},{24,28},{28,24},{1,5},{5... | collective-permute-start | bytes 3145736 | tf_op jit(solution)/shard_map/ppermute | solution.py:178
  71.2 1.0 copy-start.5
  73.4 1.0 copy-start.7
  74.9 1.0 copy-start.9
  75.9 1.6 %copy-start.1 = (bf16[2048,512]{1,0:T(8,128)(2,1)S(1)}, bf16[2048,512]{1,0:T(8,128)(2,1)}, u32[]{:S(2)}) copy-start(bf16[2048,512]{1,0:T(8,128)(2,1)} %own_ref.1) | copy-start | bytes 6291460
  77.5 1.2 %copy-start.6 = (bf16[1024,512]{1,0:T(8,128)(2,1)S(1)}, bf16[1024,512]{1,0:T(8,128)(2,1)}, u32[]{:S(2)}) copy-start(bf16[1024,512]{1,0:T(8,128)(2,1)} %copy-done.5) | copy-start | bytes 3145732
  78.7 1.2 %copy-start.8 = (bf16[1024,512]{1,0:T(8,128)(2,1)S(1)}, bf16[1024,512]{1,0:T(8,128)(2,1)}, u32[]{:S(2)}) copy-start(bf16[1024,512]{1,0:T(8,128)(2,1)} %copy-done.7) | copy-start | bytes 3145732
  79.9 1.2 %copy-start.10 = (bf16[1024,512]{1,0:T(8,128)(2,1)S(1)}, bf16[1024,512]{1,0:T(8,128)(2,1)}, u32[]{:S(2)}) copy-start(bf16[1024,512]{1,0:T(8,128)(2,1)} %copy-done.9) | copy-start | bytes 3145732
  81.2 1.0 %copy-start.11 = (bf16[512,512]{1,0:T(8,128)(2,1)S(1)}, bf16[512,512]{1,0:T(8,128)(2,1)}, u32[]{:S(2)}) copy-start(bf16[512,512]{1,0:T(8,128)(2,1)} %constant.147.clone.gh_ref) | copy-start | bytes 1572868
  82.2 1.0 %copy-start.12 = (bf16[512,512]{1,0:T(8,128)(2,1)S(1)}, bf16[512,512]{1,0:T(8,128)(2,1)}, u32[]{:S(2)}) copy-start(bf16[512,512]{1,0:T(8,128)(2,1)} %constant.148.clone.gl_ref) | copy-start | bytes 1572868
  88.3 0.8 copy-start.2
  89.1 12.9 %all-to-all-start.2 = ((bf16[4,128,512]{2,1,0:T(8,128)(2,1)}), bf16[4,128,512]{2,1,0:T(8,128)(2,1)S(1)}, u32[]{:S(2)}, u32[]{:S(2)}) async-start(bf16[4,128,512]{2,1,0:T(8,128)(2,1)} %copy-done.2), calls=%async_computation.2 | async-start | bytes 1048576 | tf_op jit(solution)/shard_map/all_to_all | solution.py:236

commit v2 on v1

--- a/solution.py
+++ b/solution.py
@@ -66,11 +66,17 @@
     return terms
 
 
-def position_kernel(x_ref, m_ref, tw_c, tw_s, th_ref, tl_ref, o_ref, lh_ref, ll_ref):
+def position_kernel(x_ref, m_ref, tw_c, tw_s, th_in, tl_in, o_ref, lh_ref, ll_ref, th_ref, tl_ref, sems):
     rows, chans, seg = x_ref.shape
     pairs = chans // 2
     cols = o_ref.shape[1]
     kb = o_ref.shape[2]
+    tables = (
+        pltpu.make_async_copy(th_in, th_ref, sems.at[0]),
+        pltpu.make_async_copy(tl_in, tl_ref, sems.at[1]),
+    )
+    for copy in tables:
+        copy.start()
     mask = m_ref[...]
     evens, odds = [], []
     for r in range(rows):
@@ -103,6 +109,8 @@
                 mask * tr + (1.0 - mask) * ti,
             )
     width = o_ref.shape[3]
+    for copy in tables:
+        copy.wait()
     for c in range(cols):
         lh, ll = lh_ref[c * width : (c + 1) * width], ll_ref[c * width : (c + 1) * width]
         th = th_ref[...]
@@ -111,13 +119,19 @@
             o_ref[r, c] = z[r * kb : (r + 1) * kb]
 
 
-def output_kernel(at_ref, z_ref, gh_ref, gl_ref, own_ref, *refs):
+def output_kernel(at_ref, z_ref, gh_in, gl_in, own_ref, *refs):
     rows, cols, kb, width = z_ref.shape
     total = own_ref.shape[0]
     mine, other = refs[: cols - 1], refs[cols - 1 : 2 * (cols - 1)]
-    o_ref, zh_ref, zl_ref, sh_ref, own_v, mine_v, other_v, sems = refs[2 * (cols - 1) :]
+    o_ref, zh_ref, zl_ref, sh_ref, own_v, mine_v, other_v, gh_ref, gl_ref, sems = refs[2 * (cols - 1) :]
     chans = total // (rows * cols)
     jb = width // chans
+    tables = (
+        pltpu.make_async_copy(gh_in, gh_ref, sems.at[2 * cols - 1]),
+        pltpu.make_async_copy(gl_in, gl_ref, sems.at[2 * cols]),
+    )
+    for copy in tables:
+        copy.start()
     own_copy = pltpu.make_async_copy(own_ref, own_v, sems.at[0])
     own_copy.start()
     copies = []
@@ -138,6 +152,8 @@
                 zh_ref[jj * kb : (jj + 1) * kb, lane : lane + chans] = high[:, jj * chans : (jj + 1) * chans]
                 zl_ref[jj * kb : (jj + 1) * kb, lane : lane + chans] = low[:, jj * chans : (jj + 1) * chans]
     few = jb * kb
+    for copy in tables:
+        copy.wait()
     for g in range(GROUPS):
         cut = slice(g * GROUP_DIM, (g + 1) * GROUP_DIM)
         zh, zl = zh_ref[:, cut], zl_ref[:, cut]
@@ -195,12 +211,14 @@
     phase = 2 * np.pi * ((s_at[:, None] * s_at[None, :]) % seg) / seg
     th, tl = two_parts(np.concatenate([np.cos(phase), np.sin(phase)], axis=1))
     in_vmem = pl.BlockSpec(memory_space=pltpu.VMEM)
+    in_hbm = pl.BlockSpec(memory_space=pltpu.HBM)
     spread = pl.pallas_call(
         position_kernel,
         out_shape=jax.ShapeDtypeStruct((rows, cols, kb, jb * chans), F32),
-        in_specs=[in_vmem] * 6,
-        scratch_shapes=[pltpu.VMEM((rows * chans, 2 * seg), BF)] * 2,
-        compiler_params=pltpu.CompilerParams(vmem_limit_bytes=20 * 1024 * 1024),
+        in_specs=[in_vmem] * 4 + [in_hbm] * 2,
+        scratch_shapes=[pltpu.VMEM((rows * chans, 2 * seg), BF)] * 2
+        + [pltpu.VMEM((seg, 2 * seg), BF)] * 2
+        + [pltpu.SemaphoreType.DMA((2,))],
         name="positions",
     )(whole, mask, np.cos(twist).astype(np.float32), np.sin(twist).astype(np.float32), th, tl)
     flat = spread.reshape(rows * cols, kb, jb * chans)
@@ -216,21 +234,21 @@
     gh, gl = two_parts(grid_table / math.sqrt(length * GROUP_DIM))
     places = jnp.stack([half, col]).astype(jnp.int32)
     few = jb * kb
-    anywhere = pl.BlockSpec(memory_space=pl.ANY)
     out = pl.pallas_call(
         output_kernel,
         out_shape=jax.ShapeDtypeStruct((cols, few, out_cols), BF),
-        in_specs=[pl.BlockSpec(memory_space=pltpu.SMEM), in_vmem, in_vmem, in_vmem]
-        + [anywhere] * (2 * cols - 1),
+        in_specs=[pl.BlockSpec(memory_space=pltpu.SMEM), in_vmem]
+        + [in_hbm] * (2 * cols + 1),
         scratch_shapes=[pltpu.VMEM((few, dim), BF)] * 2
         + [
             pltpu.VMEM((2, 2 * few, dim // 2), BF),
             pltpu.VMEM((dim, out_cols), BF),
             pltpu.VMEM((cols - 1, dim // 2, out_cols), BF),
             pltpu.VMEM((cols - 1, dim // 2, out_cols), BF),
-            pltpu.SemaphoreType.DMA((2 * cols - 1,)),
+            pltpu.VMEM((GROUP_DIM, GROUP_DIM), BF),
+            pltpu.VMEM((GROUP_DIM, GROUP_DIM), BF),
+            pltpu.SemaphoreType.DMA((2 * cols + 1,)),
         ],
-        compiler_params=pltpu.CompilerParams(vmem_limit_bytes=26 * 1024 * 1024),
         name="outputs",
     )(places, mixed_in, gh, gl, out_weight, *fetched, *swapped)
     gathered = lax.all_to_all(out, "col", split_axis=0, concat_axis=0, tiled=True)

time: 104 us -> 97.8 us (0.940)
  local copies, waits for them, and re-layouts: 17.4 us -> 6.66 us
  Pallas kernels: 9.82 us -> 14.1 us
  other arithmetic: 0.11 us -> 1.27 us
    unnamed x30 -> x10, local copies, waits for them, and re-layouts: 15.1 us -> 4.35 us
    pallas_call x1, Pallas kernels: 4.8 us -> 7.01 us  [body(): pl.pallas_call(position_kernel, out_shape=jax.ShapeDtypeStruct((rows, col...]
    pallas_call x1, Pallas kernels: 5.01 us -> 7.14 us  [body(): pl.pallas_call(output_kernel, out_shape=jax.ShapeDtypeStruct((cols, few,...]
  transfers between devices with their start and end apart: 9 -> 9, of which waited for: 7 -> 7; matrix products, arithmetic and copies ran while one was open for 2% -> 4% of each run, Pallas kernels for 5% -> 7%
where the time goes in v2:
time: 97.8 us; the launch traced here: 97.3 us
  waiting for transfers between devices  55.4 us (57%)
  starting transfers between devices  17.3 us (18%)
  Pallas kernels  14.1 us (14%)
  local copies, waits for them, and re-layouts  6.66 us (7%)
  matrix products  2.55 us (3%)
  other arithmetic  1.27 us (1%)
    ppermute x3, waiting for transfers between devices, body(): fetched.append(lax.ppermute(own, 'col', [(c, c ^ d) for c in range(cols)]))  35.1 us
    all_to_all x1, waiting for transfers between devices, body(): lax.all_to_all(out, 'col', split_axis=0, concat_axis=0, tiled=True)  9 us
    all_to_all x1, waiting for transfers between devices, body(): lax.all_to_all(turned, 'row', split_axis=0, concat_axis=0, tiled=True)  8.92 us
    pallas_call x1, Pallas kernels, body(): pl.pallas_call(output_kernel, out_shape=jax.ShapeDtypeStruct((cols, few,...  7.14 us
    pallas_call x1, Pallas kernels, body(): pl.pallas_call(position_kernel, out_shape=jax.ShapeDtypeStruct((rows, col...  7.01 us
    all_to_all x1, starting transfers between devices, body(): lax.all_to_all(turned, 'row', split_axis=0, concat_axis=0, tiled=True)  6.35 us
    unnamed x10, local copies, waits for them, and re-layouts  4.35 us
    all_to_all x1, starting transfers between devices, body(): lax.all_to_all(out, 'col', split_axis=0, concat_axis=0, tiled=True)  3.86 us
  transfers between devices with their start and end apart: 9, of which 7 were waited for; matrix products, arithmetic and copies ran while one was open for 4% of the time, Pallas kernels for 7%

profile of v2, /device:TPU:0, one launch (start us, length us, event | category | flops | bytes accessed | tf_op | source)
XLA Modules:
  0.0 97.3 jit_solution(14724107041251627883)
XLA Ops:
  0.0 1.6 %copy-done = bf16[512,2048]{1,0:T(8,128)(2,1)S(1)} copy-done((bf16[512,2048]{1,0:T(8,128)(2,1)S(1)}, bf16[512,2048]{1,0:T(8,128)(2,1)}, u32[]{:S(2)}) %copy-start) | copy-done | bytes 2097176
  1.6 1.3 %convolution_convert_fusion.1 = bf16[512,512]{1,0:T(8,128)(2,1)} fusion(bf16[512,2048]{1,0:T(8,128)(2,1)S(1)} %copy-done, s32[]{:T(128)S(6)} %select_n.109, s32[512]{0:T(512)S(1)} %select_select_fusion), kind=kOutput, calls=%fused_computation.1 | convolution fusion | flops 268959744 | bytes 1050628 | tf_op jit(solution)/shard_map/dot_general | solution.py:31
  2.9 6.4 %all-to-all-start = ((bf16[8,64,512]{2,1,0:T(8,128)(2,1)}), bf16[8,64,512]{2,1,0:T(8,128)(2,1)S(1)}, u32[]{:S(2)}, u32[]{:S(2)}) async-start(bf16[8,64,512]{2,1,0:T(8,128)(2,1)} %bitcast.2), calls=%async_computation | async-start | bytes 1048576 | tf_op jit(solution)/shard_map/all_to_all | solution.py:205
  9.2 2.3 %constant_dynamic-slice_fusion = bf16[1024,512]{1,0:T(8,128)(2,1)} fusion(bf16[2048,512]{1,0:T(8,128)(2,1)} %own_ref.1, s32[]{:T(128)S(6)} %select_n.111), kind=kLoop, calls=%fused_computation.48 | loop fusion | bytes 2097156 | tf_op jit(solution)/shard_map/dynamic_slice | solution.py:190
  11.5 1.5 %collective-permute-start = (bf16[1024,512]{1,0:T(8,128)(2,1)}, bf16[1024,512]{1,0:T(8,128)(2,1)}, u32[]{:S(2)}, u32[]{:S(2)}) collective-permute-start(bf16[1024,512]{1,0:T(8,128)(2,1)} %constant_dynamic-slice_fusion), channel_id=1, source_target_pairs={{0,1},{1,0},{2,3},{3,2},{4,5},{5,4},{6,7},{7,6},{8,9},{9,8},{10,11... | collective-permute-start | bytes 3145736 | tf_op jit(solution)/shard_map/ppermute | solution.py:193
  13.0 1.5 %collective-permute-start.1 = (bf16[1024,512]{1,0:T(8,128)(2,1)}, bf16[1024,512]{1,0:T(8,128)(2,1)}, u32[]{:S(2)}, u32[]{:S(2)}) collective-permute-start(bf16[1024,512]{1,0:T(8,128)(2,1)} %constant_dynamic-slice_fusion), channel_id=1, source_target_pairs={{0,2},{1,3},{2,0},{3,1},{4,6},{5,7},{6,4},{7,5},{8,10},{9,11},{10,... | collective-permute-start | bytes 3145736 | tf_op jit(solution)/shard_map/ppermute | solution.py:193
  14.5 0.5 collective-permute-start.2
  15.0 0.6 fusion.7.m_ref
  15.6 8.9 %all-to-all-done.x_ref = bf16[8,64,512]{2,1,0:T(8,128)(2,1)S(1)} async-done(((bf16[8,64,512]{2,1,0:T(8,128)(2,1)}), bf16[8,64,512]{2,1,0:T(8,128)(2,1)S(1)}, u32[]{:S(2)}, u32[]{:S(2)}) %all-to-all-start) | async-done | bytes 524320 | tf_op jit(solution)/shard_map/all_to_all | solution.py:205
  24.6 0.8 copy-done.2
  25.3 7.0 %positions.1 = f32[8,4,64,128]{3,2,1,0:T(8,128)} custom-call(bf16[8,64,512]{2,1,0:T(8,128)(2,1)} %copy-done.2, f32[32,1]{1,0:T(8,128)} %fusion.7.m_ref, f32[8,512]{1,0:T(8,128)} %constant.143.clone.tw_c, f32[8,512]{1,0:T(8,128)} %constant.144.clone.tw_s, bf16[512,1024]{1,0:T(8,128)(2,1)} %constant.145.clone.th_in, bf16[512,1024]{1,0:T(8,128)(2,1)} %constant.146.clone.tl_in), custom_call_target="tpu_custom_call" | custom-call | tf_op jit(solution)/shard_map/positions/pallas_call | solution.py:215
  32.4 3.5 %all-to-all-start.1 = ((f32[32,64,128]{2,1,0:T(8,128)}), f32[32,64,128]{2,1,0:T(8,128)S(1)}, u32[]{:S(2)}, u32[]{:S(2)}) async-start(f32[32,64,128]{2,1,0:T(8,128)} %bitcast.7), calls=%async_computation.1 | async-start | bytes 2097152 | tf_op jit(solution)/shard_map/all_to_all | solution.py:225
  35.9 2.0 %collective-permute-done.refs_0_ = bf16[1024,512]{1,0:T(8,128)(2,1)} collective-permute-done((bf16[1024,512]{1,0:T(8,128)(2,1)}, bf16[1024,512]{1,0:T(8,128)(2,1)}, u32[]{:S(2)}, u32[]{:S(2)}) %collective-permute-start) | collective-permute-done | bytes 1048608 | tf_op jit(solution)/shard_map/ppermute | solution.py:193
  37.9 32.7 %collective-permute-done.1.refs_1_ = bf16[1024,512]{1,0:T(8,128)(2,1)} collective-permute-done((bf16[1024,512]{1,0:T(8,128)(2,1)}, bf16[1024,512]{1,0:T(8,128)(2,1)}, u32[]{:S(2)}, u32[]{:S(2)}) %collective-permute-start.1) | collective-permute-done | bytes 1048608 | tf_op jit(solution)/shard_map/ppermute | solution.py:193
  70.6 0.4 collective-permute-done.2.refs_2_
  71.1 0.6 pad_add_fusion.at_ref
  71.7 1.7 %collective-permute-done.4.refs_4_ = bf16[1024,512]{1,0:T(8,128)(2,1)S(1)} collective-permute-done((bf16[1024,512]{1,0:T(8,128)(2,1)}, bf16[1024,512]{1,0:T(8,128)(2,1)S(1)}, u32[]{:S(2)}, u32[]{:S(2)}) %collective-permute-start.4) | collective-permute-done | bytes 1048608 | tf_op jit(solution)/shard_map/ppermute | solution.py:194
  73.4 1.0 %copy-done.4 = bf16[1024,512]{1,0:T(8,128)(2,1)} copy-done((bf16[1024,512]{1,0:T(8,128)(2,1)}, bf16[1024,512]{1,0:T(8,128)(2,1)S(1)}, u32[]{:S(2)}) %copy-start.4) | copy-done | bytes 1048600
  74.4 0.6 collective-permute-done.5.refs_5_
  75.1 1.0 %copy-done.1 = f32[32,64,128]{2,1,0:T(8,128)} copy-done((f32[32,64,128]{2,1,0:T(8,128)}, f32[32,64,128]{2,1,0:T(8,128)S(1)}, u32[]{:S(2)}) %copy-start.1) | copy-done | bytes 1048600
  76.1 7.1 %outputs.1 = bf16[4,128,512]{2,1,0:T(8,128)(2,1)} custom-call(s32[2]{0:T(128)} %pad_add_fusion.at_ref, f32[8,4,64,128]{3,2,1,0:T(8,128)} %bitcast.8, bf16[512,512]{1,0:T(8,128)(2,1)} %constant.147.clone.gh_in, bf16[512,512]{1,0:T(8,128)(2,1)} %constant.148.clone.gl_in, bf16[2048,512]{1,0:T(8,128)(2,1)} %own_ref.1, ...), custom_call_target="tpu_custom_call" | custom-call | tf_op jit(solution)/shard_map/outputs/pallas_call | solution.py:237
  83.2 3.9 %all-to-all-start.2 = ((bf16[4,128,512]{2,1,0:T(8,128)(2,1)}), bf16[4,128,512]{2,1,0:T(8,128)(2,1)S(1)}, u32[]{:S(2)}, u32[]{:S(2)}) async-start(bf16[4,128,512]{2,1,0:T(8,128)(2,1)} %outputs.1), calls=%async_computation.2 | async-start | bytes 1048576 | tf_op jit(solution)/shard_map/all_to_all | solution.py:254
  87.1 9.0 %all-to-all-done.2 = bf16[4,128,512]{2,1,0:T(8,128)(2,1)S(1)} async-done(((bf16[4,128,512]{2,1,0:T(8,128)(2,1)}), bf16[4,128,512]{2,1,0:T(8,128)(2,1)S(1)}, u32[]{:S(2)}, u32[]{:S(2)}) %all-to-all-start.2) | async-done | bytes 524320 | tf_op jit(solution)/shard_map/all_to_all | solution.py:254
  96.1 1.3 %convolution_convert_fusion = bf16[512,512]{1,0:T(8,128)(2,1)} fusion(bf16[512,512]{1,0:T(8,128)(2,1)S(1)} %bitcast.9, s32[512]{0:T(512)S(1)} %fusion.13), kind=kOutput, calls=%fused_computation | convolution fusion | flops 268959744 | bytes 1050624 | tf_op jit(solution)/shard_map/dot_general | solution.py:35
  (13 shorter events, 0.1 us)
Async XLA Ops:
  0.0 1.6 %copy-start = (bf16[512,2048]{1,0:T(8,128)(2,1)S(1)}, bf16[512,2048]{1,0:T(8,128)(2,1)}, u32[]{:S(2)}) copy-start(bf16[512,2048]{1,0:T(8,128)(2,1)} %param.8) | copy-start | bytes 6291460
  2.9 21.7 %all-to-all-start = ((bf16[8,64,512]{2,1,0:T(8,128)(2,1)}), bf16[8,64,512]{2,1,0:T(8,128)(2,1)S(1)}, u32[]{:S(2)}, u32[]{:S(2)}) async-start(bf16[8,64,512]{2,1,0:T(8,128)(2,1)} %bitcast.2), calls=%async_computation | async-start | bytes 1048576 | tf_op jit(solution)/shard_map/all_to_all | solution.py:205
  11.5 26.3 %collective-permute-start = (bf16[1024,512]{1,0:T(8,128)(2,1)}, bf16[1024,512]{1,0:T(8,128)(2,1)}, u32[]{:S(2)}, u32[]{:S(2)}) collective-permute-start(bf16[1024,512]{1,0:T(8,128)(2,1)} %constant_dynamic-slice_fusion), channel_id=1, source_target_pairs={{0,1},{1,0},{2,3},{3,2},{4,5},{5,4},{6,7},{7,6},{8,9},{9,8},{10,11... | collective-permute-start | bytes 3145736 | tf_op jit(solution)/shard_map/ppermute | solution.py:193
  13.0 57.5 %collective-permute-start.1 = (bf16[1024,512]{1,0:T(8,128)(2,1)}, bf16[1024,512]{1,0:T(8,128)(2,1)}, u32[]{:S(2)}, u32[]{:S(2)}) collective-permute-start(bf16[1024,512]{1,0:T(8,128)(2,1)} %constant_dynamic-slice_fusion), channel_id=1, source_target_pairs={{0,2},{1,3},{2,0},{3,1},{4,6},{5,7},{6,4},{7,5},{8,10},{9,11},{10,... | collective-permute-start | bytes 3145736 | tf_op jit(solution)/shard_map/ppermute | solution.py:193
  14.5 56.5 %collective-permute-start.2 = (bf16[1024,512]{1,0:T(8,128)(2,1)}, bf16[1024,512]{1,0:T(8,128)(2,1)}, u32[]{:S(2)}, u32[]{:S(2)}) collective-permute-start(bf16[1024,512]{1,0:T(8,128)(2,1)} %constant_dynamic-slice_fusion), channel_id=1, source_target_pairs={{0,3},{1,2},{2,1},{3,0},{4,7},{5,6},{6,5},{7,4},{8,11},{9,10},{10,... | collective-permute-start | bytes 3145736 | tf_op jit(solution)/shard_map/ppermute | solution.py:193
  24.6 0.8 copy-start.2
  32.4 42.7 %all-to-all-start.1 = ((f32[32,64,128]{2,1,0:T(8,128)}), f32[32,64,128]{2,1,0:T(8,128)S(1)}, u32[]{:S(2)}, u32[]{:S(2)}) async-start(f32[32,64,128]{2,1,0:T(8,128)} %bitcast.7), calls=%async_computation.1 | async-start | bytes 2097152 | tf_op jit(solution)/shard_map/all_to_all | solution.py:225
  37.9 33.8 %collective-permute-start.3 = (bf16[1024,512]{1,0:T(8,128)(2,1)}, bf16[1024,512]{1,0:T(8,128)(2,1)S(1)}, u32[]{:S(2)}, u32[]{:S(2)}) collective-permute-start(bf16[1024,512]{1,0:T(8,128)(2,1)} %collective-permute-done.refs_0_), channel_id=1, source_target_pairs={{0,4},{4,0},{8,12},{12,8},{16,20},{20,16},{24,28},{28,24},{1,5},{5... | collective-permute-start | bytes 3145736 | tf_op jit(solution)/shard_map/ppermute | solution.py:194
  70.6 2.9 %collective-permute-start.4 = (bf16[1024,512]{1,0:T(8,128)(2,1)}, bf16[1024,512]{1,0:T(8,128)(2,1)S(1)}, u32[]{:S(2)}, u32[]{:S(2)}) collective-permute-start(bf16[1024,512]{1,0:T(8,128)(2,1)} %collective-permute-done.1.refs_1_), channel_id=1, source_target_pairs={{0,4},{4,0},{8,12},{12,8},{16,20},{20,16},{24,28},{28,24},{1,5},{5... | collective-permute-start | bytes 3145736 | tf_op jit(solution)/shard_map/ppermute | solution.py:194
  71.0 4.1 %collective-permute-start.5 = (bf16[1024,512]{1,0:T(8,128)(2,1)}, bf16[1024,512]{1,0:T(8,128)(2,1)}, u32[]{:S(2)}, u32[]{:S(2)}) collective-permute-start(bf16[1024,512]{1,0:T(8,128)(2,1)} %collective-permute-done.2.refs_2_), channel_id=1, source_target_pairs={{0,4},{4,0},{8,12},{12,8},{16,20},{20,16},{24,28},{28,24},{1,5},{5... | collective-permute-start | bytes 3145736 | tf_op jit(solution)/shard_map/ppermute | solution.py:194
  71.7 1.7 %copy-start.3 = (bf16[1024,512]{1,0:T(8,128)(2,1)}, bf16[1024,512]{1,0:T(8,128)(2,1)S(1)}, u32[]{:S(2)}) copy-start(bf16[1024,512]{1,0:T(8,128)(2,1)S(1)} %collective-permute-done.3.refs_3_) | copy-start | bytes 3145732
  73.4 1.0 %copy-start.4 = (bf16[1024,512]{1,0:T(8,128)(2,1)}, bf16[1024,512]{1,0:T(8,128)(2,1)S(1)}, u32[]{:S(2)}) copy-start(bf16[1024,512]{1,0:T(8,128)(2,1)S(1)} %collective-permute-done.4.refs_4_) | copy-start | bytes 3145732
  75.1 1.0 %copy-start.1 = (f32[32,64,128]{2,1,0:T(8,128)}, f32[32,64,128]{2,1,0:T(8,128)S(1)}, u32[]{:S(2)}) copy-start(f32[32,64,128]{2,1,0:T(8,128)S(1)} %all-to-all-done.1) | copy-start | bytes 3145732
  83.2 12.9 %all-to-all-start.2 = ((bf16[4,128,512]{2,1,0:T(8,128)(2,1)}), bf16[4,128,512]{2,1,0:T(8,128)(2,1)S(1)}, u32[]{:S(2)}, u32[]{:S(2)}) async-start(bf16[4,128,512]{2,1,0:T(8,128)(2,1)} %outputs.1), calls=%async_computation.2 | async-start | bytes 1048576 | tf_op jit(solution)/shard_map/all_to_all | solution.py:254
